TPU v7x, 32 devices: a whole 2x2x4 slice. The times are simulated.
32 devices in a mesh: sp: 8 (over z, y), tp: 4 (over x, core).
Axes of the slice: x: 2, y: 2, z: 4, core: 2. Of those that a mesh axis runs over, the one named last changes fastest.
Arguments:
- memory_queries: bfloat16 [4096, 1024], P('sp', 'tp'), may hold values from -8 to 8
- memory_keys: bfloat16 [4096, 1024], P('sp', 'tp'), may hold values from -8 to 8
- memory_values: bfloat16 [4096, 1024], P('sp', 'tp'), may hold values from -6 to 6
- input_gate_logits: float32 [8, 4096], P('tp', 'sp'), may hold values from -64 to 160
- forget_gate_logits: float32 [8, 4096], P('tp', 'sp'), may hold values from -0.1 to 20
- extra_log_decay: float32 [8, 4096], P('tp', 'sp'), may hold values from -1.4 to 0
- residual: bfloat16 [4096, 2048], P(('sp', 'tp')), may hold values from -6 to 6
- cell_output_weight: bfloat16 [1024, 2048], P('tp', 'sp'), may hold values from -0.1875 to 0.1875
- expert_norm_gain: float32 [2048], replicated, may hold values from 0.1 to 1.9
- expert_gate_weight: bfloat16 [8, 2048, 3584], P('sp', None, 'tp'), may hold values from -0.125 to 0.125
- expert_up_weight: bfloat16 [8, 2048, 3584], P('sp', None, 'tp'), may hold values from -0.125 to 0.125
- expert_down_weight: bfloat16 [8, 3584, 2048], P('sp', 'tp'), may hold values from -0.09375 to 0.09375
- routed_expert_index: int32 [4096, 2], P('sp'), may hold values from 0 to 7, as said below
- routed_expert_weight: float32 [4096, 2], P(('sp', 'tp')), may hold values from 0.1 to 1
Outputs:
- layer_out: bfloat16 [4096, 2048], P(('sp', 'tp'))
Inputs may be any that keep to these rules, and one draw needn't show every extreme that they name: `routed_expert_index`: each row names 2 different experts. In each aligned block of 128 rows (the rows of one device after the cell) no expert is named more than 40 times, and one expert is named exactly 40 times in every block.
All inputs are finite; a program needn't handle non-finite values.
Results may differ from a plain program's by a relative error of at most 0.013.
Values may be sent and summed in bfloat16 or wider, within the bound.
A program may use at most 128 MiB of HBM per device.

v0:
```python
import jax
import jax.numpy as jnp
from jax import lax
from jax.sharding import PartitionSpec as P

highest = lax.Precision.HIGHEST
lowest = -1e30
epsilon = 1e-06


def carried_in(x, axis, combine, identity):
    length, place = (lax.axis_size(axis), lax.axis_index(axis))
    everything = jax.tree.map(lambda part: lax.all_gather(part, axis), x)
    start = jax.tree.map(
        lambda part, zero: jnp.broadcast_to(jnp.asarray(zero, part.dtype), part.shape), x, identity
    )

    def turn(k, before):
        reached = k < place
        new = combine(before, jax.tree.map(lambda part: part[k], everything))
        return jax.tree.map(lambda a, b: jnp.where(reached, a, b), new, before)

    return lax.fori_loop(0, length, turn, start)


def block_pass(memory, inputs):
    state_mat, state_norm, state_max = memory
    queries, keys_blk, values_blk, gate_in, forget_log_value = inputs
    length = gate_in.shape[-1]
    running = jnp.cumsum(forget_log_value, axis=-1)
    causal = jnp.arange(length)[:, None] >= jnp.arange(length)[None, :]
    exponent = running[:, :, None] - running[:, None, :] + gate_in[:, None, :]
    exponent = jnp.where(causal[None], exponent, -jnp.inf)
    carried = running + state_max[:, None]
    row_max = jnp.maximum(carried, jnp.max(exponent, axis=-1))
    decays = jnp.exp(exponent - row_max[:, :, None])
    carry_scale = jnp.exp(carried - row_max)
    dispatch_affinity = jnp.einsum("htk,hsk->hts", queries, keys_blk, precision=highest) * decays
    numerator = carry_scale[:, :, None] * jnp.einsum(
        "hvk,htk->htv", state_mat, queries, precision=highest
    )
    numerator = numerator + jnp.einsum(
        "hts,hsv->htv", dispatch_affinity, values_blk, precision=highest
    )
    denominator = carry_scale * jnp.einsum(
        "hk,htk->ht", state_norm, queries, precision=highest
    ) + jnp.sum(dispatch_affinity, axis=-1)
    final_log = running[:, -1]
    log_prev = final_log + state_max
    log_keep = final_log[:, None] - running + gate_in
    new_max = jnp.maximum(log_prev, jnp.max(log_keep, axis=-1))
    prev_scale = jnp.exp(log_prev - new_max)
    retain = jnp.exp(log_keep - new_max[:, None])
    new_mat = prev_scale[:, None, None] * state_mat + jnp.einsum(
        "hsv,hsk->hvk", retain[:, :, None] * values_blk, keys_blk, precision=highest
    )
    new_norm = prev_scale[:, None] * state_norm + jnp.einsum(
        "hs,hsk->hk", retain, keys_blk, precision=highest
    )
    return ((new_mat, new_norm, new_max), (numerator, denominator, row_max))


def join_states(earlier, later):
    early_log, early_mat, early_norm, early_max = earlier
    late_log, late_mat, late_norm, late_max = later
    joined_max = jnp.maximum(early_max + late_log, late_max)
    early_scale = jnp.exp(early_max + late_log - joined_max)
    late_scale = jnp.exp(late_max - joined_max)
    joined_mat = early_scale[:, None, None] * early_mat + late_scale[:, None, None] * late_mat
    joined_norm = early_scale[:, None] * early_norm + late_scale[:, None] * late_norm
    return (early_log + late_log, joined_mat, joined_norm, joined_max)


def matrix_memory_step(
    memory_queries,
    memory_keys,
    memory_values,
    input_gate_logits,
    forget_gate_logits,
    extra_log_decay,
):
    tokens_here, channels = memory_queries.shape
    heads_here = input_gate_logits.shape[0]
    head_dim = channels // heads_here

    def heads_first(tensor):
        return jnp.transpose(
            tensor.astype(jnp.float32).reshape(tokens_here, heads_here, head_dim), (1, 0, 2)
        )

    queries = heads_first(memory_queries) * head_dim ** (-0.5)
    forget_log_value = jax.nn.log_sigmoid(forget_gate_logits) + extra_log_decay
    block_size = min(tokens_here, 256)
    block_count = tokens_here // block_size

    def split_blocks(tensor):
        return jnp.moveaxis(
            tensor.reshape((heads_here, block_count, block_size) + tensor.shape[2:]), 1, 0
        )

    def join_blocks(tensor):
        return jnp.moveaxis(tensor, 0, 1).reshape((heads_here, tokens_here) + tensor.shape[3:])

    empty_state = (
        jnp.zeros((heads_here, head_dim, head_dim), jnp.float32),
        jnp.zeros((heads_here, head_dim), jnp.float32),
        jnp.full((heads_here,), lowest, jnp.float32),
    )
    members = (
        queries,
        heads_first(memory_keys),
        heads_first(memory_values),
        input_gate_logits,
        forget_log_value,
    )
    end_state, pieces = lax.scan(
        block_pass, empty_state, tuple((split_blocks(member) for member in members))
    )
    numerator, denominator, row_max = (join_blocks(member) for member in pieces)
    running = jnp.cumsum(forget_log_value, axis=-1)
    identity = (jnp.zeros((heads_here,), jnp.float32),) + empty_state
    incoming = carried_in((running[:, -1],) + tuple(end_state), "sp", join_states, identity)
    prior_mat, prior_norm, prior_max = incoming[1:]
    reached = running + prior_max[:, None]
    joined = jnp.maximum(row_max, reached)
    local_scale = jnp.exp(row_max - joined)
    carry_scale = jnp.exp(reached - joined)
    numerator = local_scale[:, :, None] * numerator + carry_scale[:, :, None] * jnp.einsum(
        "hvk,htk->htv", prior_mat, queries, precision=highest
    )
    denominator = local_scale * denominator + carry_scale * jnp.einsum(
        "hk,htk->ht", prior_norm, queries, precision=highest
    )
    guarded = jnp.maximum(jnp.abs(denominator), jnp.exp(-joined))
    return ((numerator / guarded[:, :, None]).astype(jnp.bfloat16), heads_here, head_dim)


def slot_index(ids, experts, capacity):
    flat_ids = ids.reshape(-1)
    matches = (flat_ids[:, None] == jnp.arange(experts, dtype=jnp.int32)[None, :]).astype(jnp.int32)
    before = jnp.cumsum(matches, axis=0) - matches
    return flat_ids * capacity + jnp.sum(before * matches, axis=1)


def local(
    memory_queries,
    memory_keys,
    memory_values,
    input_gate_logits,
    forget_gate_logits,
    extra_log_decay,
    residual,
    cell_output_weight,
    expert_norm_gain,
    expert_gate_weight,
    expert_up_weight,
    expert_down_weight,
    routed_expert_index,
    routed_expert_weight,
):
    hidden, heads_here, head_dim = matrix_memory_step(
        memory_queries,
        memory_keys,
        memory_values,
        input_gate_logits,
        forget_gate_logits,
        extra_log_decay,
    )
    weight_piece = lax.all_gather(cell_output_weight, "sp", axis=1, tiled=True)
    shaped = weight_piece.reshape(heads_here, head_dim, weight_piece.shape[1])
    partial_rows = jnp.einsum(
        "htd,hdc->tc", hidden, shaped, preferred_element_type=jnp.float32
    ).astype(jnp.bfloat16)
    projected = lax.psum_scatter(
        partial_rows.astype(jnp.float32).astype(jnp.bfloat16), "tp", scatter_dimension=0, tiled=True
    ).astype(jnp.float32)
    mixed_rows = (residual.astype(jnp.float32) + projected).astype(jnp.bfloat16)
    mixed_wide = mixed_rows.astype(jnp.float32)
    norm_scale = lax.rsqrt(jnp.mean(mixed_wide * mixed_wide, axis=-1, keepdims=True) + epsilon)
    normed = (mixed_wide * norm_scale * expert_norm_gain).astype(jnp.bfloat16)
    sp_size = lax.axis_size("sp")
    row_count, model_width = residual.shape
    top_count = routed_expert_index.shape[1]
    experts = sp_size * expert_gate_weight.shape[0]
    assigned = row_count * top_count
    capacity = max(2, assigned * 5 // (4 * experts))
    own_ids = lax.dynamic_slice_in_dim(
        routed_expert_index, lax.axis_index("tp") * row_count, row_count, 0
    )
    own_slots = slot_index(own_ids, experts, capacity)
    zero_row = jnp.zeros((1, model_width), jnp.bfloat16)
    padded = jnp.concatenate([normed, zero_row], axis=0)
    slot_table = jnp.full((experts * capacity,), row_count, jnp.int32)
    slot_table = slot_table.at[own_slots].set(jnp.arange(assigned, dtype=jnp.int32) // top_count)
    arrived = lax.all_gather(
        lax.all_to_all(
            padded[slot_table.reshape(experts, 1, capacity)],
            "sp",
            split_axis=0,
            concat_axis=0,
            tiled=True,
        ),
        "tp",
        axis=1,
        tiled=True,
    )
    sources, owners, slot_span, width_in = arrived.shape
    flat_rows = arrived.reshape(-1, width_in)
    gate_pre = jnp.dot(flat_rows, expert_gate_weight[0], preferred_element_type=jnp.float32)
    up_pre = jnp.dot(flat_rows, expert_up_weight[0], preferred_element_type=jnp.float32)
    hidden_act = (jax.nn.silu(gate_pre) * up_pre).astype(jnp.bfloat16)
    group_term = jnp.dot(hidden_act, expert_down_weight[0], preferred_element_type=jnp.float32)
    group_term = lax.optimization_barrier(group_term.astype(jnp.bfloat16)).astype(jnp.float32)
    summed = lax.psum_scatter(
        group_term.reshape(sources, owners, slot_span, width_in).astype(jnp.bfloat16),
        "tp",
        scatter_dimension=1,
        tiled=True,
    )
    returned = lax.all_to_all(summed, "sp", split_axis=0, concat_axis=0, tiled=True)
    picked = returned.reshape(experts * capacity, model_width)[own_slots]
    picked = picked.reshape(row_count, top_count, model_width).astype(jnp.float32)
    routed_sum = jnp.sum(picked * routed_expert_weight[:, :, None], axis=1)
    return (mixed_wide + routed_sum).astype(jnp.bfloat16)


def solution(mesh):
    return jax.shard_map(
        local,
        mesh=mesh,
        in_specs=(
            P("sp", "tp"),
            P("sp", "tp"),
            P("sp", "tp"),
            P("tp", "sp"),
            P("tp", "sp"),
            P("tp", "sp"),
            P(("sp", "tp"), None),
            P("tp", "sp"),
            P(),
            P("sp", None, "tp"),
            P("sp", None, "tp"),
            P("sp", "tp", None),
            P("sp", None),
            P(("sp", "tp"), None),
        ),
        out_specs=P(("sp", "tp"), None),
        check_vma=False,
    )
```

profile of v0, /device:TPU:0, one launch (start us, length us, event | category | flops | bytes accessed | tf_op | source)
XLA Modules:
  0.0 404.9 jit_solution(8255470432722626242)
XLA Ops:
  6.6 1.1 copy.56
  8.0 1.1 copy.54
  9.9 11.3 %while.39 = (s32[]{:T(128)}, f32[2,128,128]{2,1,0:T(8,128)S(1)}, f32[2,128]{1,0:T(2,128)S(1)}, f32[2]{0:T(128)S(1)}, f32[2,2,256,128]{3,2,0,1:T(8,128)S(1)}, /*i...) while((s32[]{:T(128)}, f32[2,128,128]{2,1,0:T(8,128)S(1)}, ...), condition=%wide.region_6.7_spmd.clone, body=%wide.region_0.6_spmd.clone.sunk | while | flops 607329536 | bytes 4625314 | solution.py:116
  9.9 0.6 reduce-window.38
  11.7 0.6 fusion.123
  13.6 1.0 fusion.125
  14.8 0.7 convolution_add_fusion.3
  15.6 0.6 reduce-window.38
  17.3 0.6 fusion.123
  19.3 1.0 fusion.125
  20.4 0.7 convolution_add_fusion.3
  21.2 0.6 copy-done
  21.9 0.7 all-gather.9.cloned.1.call-update
  22.7 0.6 reduce-window.22
  23.9 0.7 dynamic-slice
  25.6 23.2 %all-reduce.4 = (f32[16]{0:T(128)S(1)}, f32[16]{0:T(128)S(1)}) all-reduce(f32[16]{0:T(128)S(1)} %bitcast_dynamic-update-slice_fusion.1, f32[16]{0:T(128)S(1)} %dynamic-update-slice.1), channel_id=2, replica_groups=mesh['sp'=8,'tp'=4] {'sp'}, use_global_device_ids=true, to_apply=%add.1 | all-reduce | flops 32 | bytes 256
  49.0 16.4 %all-gather.4 = f32[8,2,128]{2,1,0:T(2,128)S(1)} all-gather(f32[1,2,128]{2,1,0:T(2,128)S(1)} %bitcast.293), channel_id=5, replica_groups=mesh['sp'=8,'tp'=4] {'sp'}, dimensions={0}, use_global_device_ids=true | all-gather | bytes 9216 | tf_op jit(solution)/shard_map/all_gather | solution.py:13
  65.4 9.0 %while.40 = (s32[]{:T(128)}, f32[2,128,128]{2,1,0:T(8,128)S(1)}, f32[2,128]{1,0:T(2,128)S(1)}, f32[2]{0:T(128)S(1)}, s32[]{:T(128)}, /*index=5*/f32[8,2]{1,0:T(8...) while((s32[]{:T(128)}, f32[2,128,128]{2,1,0:T(8,128)S(1)}, ...), condition=%wide.region_10.11_spmd.clone, body=%wide.region_9.10_spmd.clone.sunk | while | flops 165138 | bytes 396541 | solution.py:23
  65.5 1.0 fusion.126
  66.6 1.0 fusion.126
  67.7 1.0 fusion.126
  68.8 1.0 fusion.126
  69.9 1.0 fusion.126
  71.1 1.0 fusion.126
  72.2 1.0 fusion.126
  73.3 1.0 fusion.126
  75.1 1.2 fusion.47
  76.3 29.1 %all-gather.9.cloned.1.call-done = bf16[256,2048]{1,0:T(8,128)(2,1)} async-done(((bf16[256,256]{1,0:T(8,128)(2,1)}), bf16[256,2048]{1,0:T(8,128)(2,1)}) %all-gather.9.cloned.1.call-update) | async-done | bytes 1048592 | tf_op jit(solution)/shard_map/all_gather | solution.py:169
  105.3 3.3 bitcast_convert_fusion
  108.7 0.7 broadcast_multiply_fusion
  111.0 1.4 scatter_custom_fusion
  112.6 26.4 %reduce-scatter.3.cloned.1.call-done = bf16[128,2048]{1,0:T(8,128)(2,1)} async-done(((bf16[512,2048]{1,0:T(8,128)(2,1)}), bf16[128,2048]{1,0:T(8,128)(2,1)}) %reduce-scatter.3.cloned.1.call-update) | async-done | bytes 524304 | tf_op jit(solution)/shard_map/reduce_scatter | solution.py:174
  139.0 1.3 fusion.48
  140.3 1.3 fusion.50
  141.6 2.4 gather_fusion
  144.0 36.6 %all_to_all.10 = bf16[8,1,40,2048]{3,2,1,0:T(8,128)(2,1)} all-to-all(bf16[8,1,40,2048]{3,2,1,0:T(8,128)(2,1)S(1)} %bitcast.275), channel_id=1, replica_groups=mesh['sp'=8,'tp'=4] {'sp'}, dimensions={0} | all-to-all | bytes 2621440 | tf_op jit(solution)/shard_map/all_to_all | solution.py:196
  180.9 38.4 %all-gather.11.cloned.1.call-done = bf16[8,4,40,2048]{3,2,1,0:T(8,128)(2,1)} async-done(((bf16[8,1,40,2048]{3,2,1,0:T(8,128)(2,1)}), bf16[8,4,40,2048]{3,2,1,0:T(8,128)(2,1)}) %all-gather.11.cloned.1.call-update) | async-done | bytes 5242896 | tf_op jit(solution)/shard_map/all_gather | solution.py:195
  219.3 10.0 %fusion.43 = f32[1280,896]{1,0:T(8,128)} fusion(bf16[1280,2048]{1,0:T(8,128)(2,1)} %bitcast.302, bf16[1,2048,896]{2,1,0:T(8,128)(2,1)} %param.27), kind=kOutput, calls=%fused_computation.81 | convolution fusion | flops 4697620480 | bytes 13500416 | tf_op jit(solution)/shard_map/dot_general | solution.py:209
  229.3 17.6 %convolution_convert_fusion = bf16[1280,2048]{1,0:T(8,128)(2,1)} fusion(bf16[1,896,2048]{2,1,0:T(8,128)(2,1)} %param.29, f32[1280,896]{1,0:T(8,128)} %fusion.43, bf16[1280,2048]{1,0:T(8,128)(2,1)} %bitcast.303, bf16[1,2048,896]{2,1,0:T(8,128)(2,1)} %param.28), kind=kOutput, calls=%fused_computation.76 | convolution fusion | flops 9404743680 | bytes 22413312 | tf_op jit(solution)/shard_map/dot_general | solution.py:212
  246.9 0.6 copy-done.9
  248.1 101.5 %all-reduce.7.cloned.1.call-done = bf16[8,4,40,2048]{3,2,1,0:T(8,128)(2,1)} async-done(((bf16[8,4,40,2048]{3,2,1,0:T(8,128)(2,1)}), bf16[8,4,40,2048]{3,2,1,0:T(8,128)(2,1)}) %all-reduce.7.cloned.1.call-update) | async-done | bytes 5242896
  349.6 3.2 constant_dynamic-slice_fusion.3
  352.8 5.5 %all-to-all-start.1 = ((bf16[8,1,40,2048]{3,2,1,0:T(8,128)(2,1)}), bf16[8,1,40,2048]{3,2,1,0:T(8,128)(2,1)S(1)}, u32[]{:S(2)}, u32[]{:S(2)}) async-start(bf16[8,1,40,2048]{3,2,1,0:T(8,128)(2,1)} %constant_dynamic-slice_fusion.3), calls=%async_computation.2 | async-start | bytes 2621440 | tf_op jit(solution)/shard_map/all_to_all | solution.py:220
  358.5 30.9 %all-to-all-done.1 = bf16[8,1,40,2048]{3,2,1,0:T(8,128)(2,1)S(1)} async-done(((bf16[8,1,40,2048]{3,2,1,0:T(8,128)(2,1)}), bf16[8,1,40,2048]{3,2,1,0:T(8,128)(2,1)S(1)}, u32[]{:S(2)}, u32[]{:S(2)}) %all-to-all-start.1) | async-done | bytes 1310752 | tf_op jit(solution)/shard_map/all_to_all | solution.py:220
  389.4 2.3 gather_fusion.1
  391.7 2.4 reshape.428
  394.2 3.2 multiply_reduce_fusion
  397.3 1.0 fusion.51
  (153 shorter events, 11.6 us)
Async XLA Ops:
  6.5 2.9 copy-start.3
  6.5 3.3 copy-start.7
  6.5 3.3 copy-start.6
  6.5 3.3 copy-start.4
  6.5 58.9 %all-gather.13.cloned.1.call-start = ((), (), s32[]{:S(2)}) async-start(), calls=%async_computation.6 | async-start | bytes 1179648 | tf_op jit(solution)/shard_map/all_gather | solution.py:13
  9.9 14.0 %copy-start.10 = (u32[32]{0:T(128)S(1)}, u32[32]{0:T(128)}, u32[]{:S(2)}) copy-start(u32[32]{0:T(128)} %constant.125) | copy-start | bytes 388
  21.2 0.7 copy-start
  21.8 83.5 %all-gather.9.cloned.1.call-start = ((), (), s32[]{:S(2)}) async-start(), calls=%async_computation.3 | async-start | bytes 1179648 | tf_op jit(solution)/shard_map/all_gather | solution.py:169
  22.6 116.4 %reduce-scatter.3.cloned.1.call-start = ((), (), s32[]{:S(2)}) async-start(), calls=%async_computation.4 | async-start | bytes 2621440 | tf_op jit(solution)/shard_map/reduce_scatter | solution.py:174
  75.1 63.9 %copy-start.1 = (bf16[128,2048]{1,0:T(8,128)(2,1)S(1)}, bf16[128,2048]{1,0:T(8,128)(2,1)}, u32[]{:S(2)}) copy-start(bf16[128,2048]{1,0:T(8,128)(2,1)} %param.24) | copy-start | bytes 1572868
  76.2 64.0 %copy-start.5 = (f32[2048]{0:T(1024)S(1)}, f32[2048]{0:T(1024)}, u32[]{:S(2)}) copy-start(f32[2048]{0:T(1024)} %param.26) | copy-start | bytes 24580
  108.6 110.7 %all-gather.11.cloned.1.call-start = ((), (), s32[]{:S(2)}) async-start(), calls=%async_computation.5 | async-start | bytes 6553600 | tf_op jit(solution)/shard_map/all_gather | solution.py:195
  180.7 168.9 %all-reduce.7.cloned.1.call-start = ((), (), s32[]{:S(2)}) async-start(), calls=%async_computation.7 | async-start | bytes 10485760
  246.9 0.7 copy-start.9
  246.9 111.4 %copy-start.8 = (f32[128,2]{0,1:T(2,128)S(1)}, f32[128,2]{0,1:T(2,128)}, u32[]{:S(2)}) copy-start(f32[128,2]{0,1:T(2,128)} %param.31) | copy-start | bytes 3076
  352.8 36.5 %all-to-all-start.1 = ((bf16[8,1,40,2048]{3,2,1,0:T(8,128)(2,1)}), bf16[8,1,40,2048]{3,2,1,0:T(8,128)(2,1)S(1)}, u32[]{:S(2)}, u32[]{:S(2)}) async-start(bf16[8,1,40,2048]{3,2,1,0:T(8,128)(2,1)} %constant_dynamic-slice_fusion.3), calls=%async_computation.2 | async-start | bytes 2621440 | tf_op jit(solution)/shard_map/all_to_all | solution.py:220
  391.7 5.6 %copy-start.2 = (bf16[128,2048]{1,0:T(8,128)(2,1)S(1)}, bf16[128,2048]{1,0:T(8,128)(2,1)}, u32[]{:S(2)}) copy-start(bf16[128,2048]{1,0:T(8,128)(2,1)} %reduce-scatter.3.cloned.1.call-done) | copy-start | bytes 1572868
Sparse Core Ops, SparseCore 0:
  22.0 43.1 all-gather.12
  67.2 38.0 all-gather.8
  108.8 30.1 reduce-scatter.2
  180.8 38.4 all-gather.10
  247.0 102.5 all-reduce.6
where the time goes:
time: 406 us; the launch traced here: 405 us
  waiting for transfers between devices  227 us (56%)
  blocking collectives  76.3 us (19%)
  matrix products  39.1 us (10%)
  other arithmetic  22 us (5%)
  local copies, waits for them, and re-layouts  20.1 us (5%)
  between operations  14.2 us (3%)
  starting transfers between devices  5.89 us (1%)
    unnamed x6, waiting for transfers between devices  102 us
    all_gather x1, waiting for transfers between devices, local(): lax.all_gather(lax.all_to_all(padded[slot_table.reshape(experts, 1, capac...  38.4 us
    all_to_all x1, blocking collectives, local(): lax.all_to_all(padded[slot_table.reshape(experts, 1, capacity)], 'sp', sp...  36.6 us
    all_to_all x1, waiting for transfers between devices, local(): lax.all_to_all(summed, 'sp', split_axis=0, concat_axis=0, tiled=True)  30.9 us
    all_gather x1, waiting for transfers between devices, local(): weight_piece = lax.all_gather(cell_output_weight, 'sp', axis=1, tiled=True)  29.1 us
    reduce_scatter x1, waiting for transfers between devices, local(): lax.psum_scatter(partial_rows.astype(jnp.float32).astype(jnp.bfloat16), '...  26.4 us
    unnamed x1, blocking collectives  23.2 us
    dot_general x1, matrix products, local(): jnp.dot(hidden_act, expert_down_weight[0], preferred_element_type=jnp.flo...  17.6 us
  transfers between devices with their start and end apart: 6, of which 5 were waited for; matrix products, arithmetic and copies ran while one was open for 4% of the time, Pallas kernels for 0%

commit v1 on v0

--- a/solution.py
+++ b/solution.py
@@ -166,7 +166,7 @@
         forget_gate_logits,
         extra_log_decay,
     )
-    weight_piece = lax.all_gather(cell_output_weight, "sp", axis=1, tiled=True)
+    weight_piece = jnp.concatenate(lax.all_gather(cell_output_weight, "sp"), 1)
     shaped = weight_piece.reshape(heads_here, head_dim, weight_piece.shape[1])
     partial_rows = jnp.einsum(
         "htd,hdc->tc", hidden, shaped, preferred_element_type=jnp.float32

time: 406 us -> 409 us (level)
    unnamed x35 -> x39, local copies, waits for them, and re-layouts: 8.66 us -> 8.64 us
where the time goes in v1:
time: 409 us; the launch traced here: 408 us
  waiting for transfers between devices  229 us (56%)
  blocking collectives  76.3 us (19%)
  matrix products  37.9 us (9%)
  local copies, waits for them, and re-layouts  22.6 us (6%)
  other arithmetic  22 us (5%)
  between operations  14.2 us (3%)
  starting transfers between devices  5.71 us (1%)
    unnamed x6, waiting for transfers between devices  102 us
    all_gather x1, waiting for transfers between devices, local(): lax.all_gather(lax.all_to_all(padded[slot_table.reshape(experts, 1, capac...  38.6 us
    all_to_all x1, blocking collectives, local(): lax.all_to_all(padded[slot_table.reshape(experts, 1, capacity)], 'sp', sp...  36.6 us
    all_gather x1, waiting for transfers between devices, local(): weight_piece = jnp.concatenate(lax.all_gather(cell_output_weight, 'sp'), 1)  31.4 us
    all_to_all x1, waiting for transfers between devices, local(): lax.all_to_all(summed, 'sp', split_axis=0, concat_axis=0, tiled=True)  30.9 us
    reduce_scatter x1, waiting for transfers between devices, local(): lax.psum_scatter(partial_rows.astype(jnp.float32).astype(jnp.bfloat16), '...  25.9 us
    unnamed x1, blocking collectives  23.3 us
    dot_general x1, matrix products, local(): jnp.dot(hidden_act, expert_down_weight[0], preferred_element_type=jnp.flo...  17.6 us
  transfers between devices with their start and end apart: 6, of which 5 were waited for; matrix products, arithmetic and copies ran while one was open for 4% of the time, Pallas kernels for 0%

profile of v1, /device:TPU:0, one launch (start us, length us, event | category | flops | bytes accessed | tf_op | source)
XLA Modules:
  0.0 408.1 jit_solution(12698315046776235370)
XLA Ops:
  6.6 1.1 copy.59
  8.0 1.1 copy.57
  9.9 11.3 %while.39 = (s32[]{:T(128)}, f32[2,128,128]{2,1,0:T(8,128)S(1)}, f32[2,128]{1,0:T(2,128)S(1)}, f32[2]{0:T(128)S(1)}, f32[2,2,256,128]{3,2,0,1:T(8,128)S(1)}, /*i...) while((s32[]{:T(128)}, f32[2,128,128]{2,1,0:T(8,128)S(1)}, ...), condition=%wide.region_6.7_spmd.clone, body=%wide.region_0.6_spmd.clone.sunk | while | flops 607329536 | bytes 4625314 | solution.py:116
  9.9 0.6 reduce-window.38
  11.7 0.6 fusion.123
  13.6 1.0 fusion.125
  14.8 0.7 convolution_add_fusion.3
  15.6 0.6 reduce-window.38
  17.3 0.6 fusion.123
  19.3 1.0 fusion.125
  20.4 0.7 convolution_add_fusion.3
  21.2 0.6 copy-done
  21.9 0.7 all-gather.14.cloned.1.call-update
  22.7 0.6 reduce-window.22
  23.9 0.7 dynamic-slice
  25.6 23.3 %all-reduce.4 = (f32[16]{0:T(128)S(1)}, f32[16]{0:T(128)S(1)}) all-reduce(f32[16]{0:T(128)S(1)} %bitcast_dynamic-update-slice_fusion.1, f32[16]{0:T(128)S(1)} %dynamic-update-slice.1), channel_id=2, replica_groups=mesh['sp'=8,'tp'=4] {'sp'}, use_global_device_ids=true, to_apply=%add.1 | all-reduce | flops 32 | bytes 256
  49.0 16.4 %all-gather.5 = f32[8,2,128]{2,1,0:T(2,128)S(1)} all-gather(f32[1,2,128]{2,1,0:T(2,128)S(1)} %bitcast.297), channel_id=5, replica_groups=mesh['sp'=8,'tp'=4] {'sp'}, dimensions={0}, use_global_device_ids=true | all-gather | bytes 9216 | tf_op jit(solution)/shard_map/all_gather | solution.py:13
  65.5 9.0 %while.40 = (s32[]{:T(128)}, f32[2,128,128]{2,1,0:T(8,128)S(1)}, f32[2,128]{1,0:T(2,128)S(1)}, f32[2]{0:T(128)S(1)}, s32[]{:T(128)}, /*index=5*/f32[8,2]{1,0:T(8...) while((s32[]{:T(128)}, f32[2,128,128]{2,1,0:T(8,128)S(1)}, ...), condition=%wide.region_10.11_spmd.clone, body=%wide.region_9.10_spmd.clone.sunk | while | flops 165138 | bytes 396541 | solution.py:23
  65.5 1.0 fusion.126
  66.6 1.0 fusion.126
  67.7 1.0 fusion.126
  68.9 1.0 fusion.126
  70.0 1.0 fusion.126
  71.1 1.0 fusion.126
  72.2 1.0 fusion.126
  73.3 1.0 fusion.126
  74.8 31.4 %all-gather.14.cloned.1.call-done = bf16[2048,256]{1,0:T(8,128)(2,1)} async-done(((bf16[256,256]{1,0:T(8,128)(2,1)}), bf16[2048,256]{1,0:T(8,128)(2,1)}) %all-gather.14.cloned.1.call-update) | async-done | bytes 1048592 | tf_op jit(solution)/shard_map/all_gather | solution.py:169
  106.2 1.8 copy.126
  108.9 1.2 fusion.47
  110.1 2.1 bitcast_convert_fusion
  112.2 0.7 broadcast_multiply_fusion
  114.6 1.6 scatter_custom_fusion
  116.3 25.9 %reduce-scatter.3.cloned.1.call-done = bf16[128,2048]{1,0:T(8,128)(2,1)} async-done(((bf16[512,2048]{1,0:T(8,128)(2,1)}), bf16[128,2048]{1,0:T(8,128)(2,1)}) %reduce-scatter.3.cloned.1.call-update) | async-done | bytes 524304 | tf_op jit(solution)/shard_map/reduce_scatter | solution.py:174
  142.2 1.3 fusion.48
  143.6 1.3 fusion.50
  144.9 2.4 gather_fusion
  147.3 36.6 %all_to_all.10 = bf16[8,1,40,2048]{3,2,1,0:T(8,128)(2,1)} all-to-all(bf16[8,1,40,2048]{3,2,1,0:T(8,128)(2,1)S(1)} %bitcast.278), channel_id=1, replica_groups=mesh['sp'=8,'tp'=4] {'sp'}, dimensions={0} | all-to-all | bytes 2621440 | tf_op jit(solution)/shard_map/all_to_all | solution.py:196
  184.0 38.6 %all-gather.10.cloned.1.call-done = bf16[8,4,40,2048]{3,2,1,0:T(8,128)(2,1)} async-done(((bf16[8,1,40,2048]{3,2,1,0:T(8,128)(2,1)}), bf16[8,4,40,2048]{3,2,1,0:T(8,128)(2,1)}) %all-gather.10.cloned.1.call-update) | async-done | bytes 5242896 | tf_op jit(solution)/shard_map/all_gather | solution.py:195
  222.6 10.0 %fusion.43 = f32[1280,896]{1,0:T(8,128)} fusion(bf16[1280,2048]{1,0:T(8,128)(2,1)} %bitcast.306, bf16[1,2048,896]{2,1,0:T(8,128)(2,1)} %param.27), kind=kOutput, calls=%fused_computation.81 | convolution fusion | flops 4697620480 | bytes 13500416 | tf_op jit(solution)/shard_map/dot_general | solution.py:209
  232.6 17.6 %convolution_convert_fusion = bf16[1280,2048]{1,0:T(8,128)(2,1)} fusion(bf16[1,896,2048]{2,1,0:T(8,128)(2,1)} %param.29, f32[1280,896]{1,0:T(8,128)} %fusion.43, bf16[1280,2048]{1,0:T(8,128)(2,1)} %bitcast.307, bf16[1,2048,896]{2,1,0:T(8,128)(2,1)} %param.28), kind=kOutput, calls=%fused_computation.76 | convolution fusion | flops 9404743680 | bytes 22413312 | tf_op jit(solution)/shard_map/dot_general | solution.py:212
  251.4 101.5 %all-reduce.7.cloned.1.call-done = bf16[8,4,40,2048]{3,2,1,0:T(8,128)(2,1)} async-done(((bf16[8,4,40,2048]{3,2,1,0:T(8,128)(2,1)}), bf16[8,4,40,2048]{3,2,1,0:T(8,128)(2,1)}) %all-reduce.7.cloned.1.call-update) | async-done | bytes 5242896
  352.9 3.2 constant_dynamic-slice_fusion.3
  356.1 5.5 %all-to-all-start.1 = ((bf16[8,1,40,2048]{3,2,1,0:T(8,128)(2,1)}), bf16[8,1,40,2048]{3,2,1,0:T(8,128)(2,1)S(1)}, u32[]{:S(2)}, u32[]{:S(2)}) async-start(bf16[8,1,40,2048]{3,2,1,0:T(8,128)(2,1)} %constant_dynamic-slice_fusion.3), calls=%async_computation.2 | async-start | bytes 2621440 | tf_op jit(solution)/shard_map/all_to_all | solution.py:220
  361.7 30.9 %all-to-all-done.1 = bf16[8,1,40,2048]{3,2,1,0:T(8,128)(2,1)S(1)} async-done(((bf16[8,1,40,2048]{3,2,1,0:T(8,128)(2,1)}), bf16[8,1,40,2048]{3,2,1,0:T(8,128)(2,1)S(1)}, u32[]{:S(2)}, u32[]{:S(2)}) %all-to-all-start.1) | async-done | bytes 1310752 | tf_op jit(solution)/shard_map/all_to_all | solution.py:220
  392.6 2.3 gather_fusion.1
  395.0 2.4 reshape.428
  397.4 3.2 multiply_reduce_fusion
  400.6 1.0 fusion.51
  (159 shorter events, 12.6 us)
Async XLA Ops:
  6.5 2.9 copy-start.5
  6.5 3.3 copy-start.9
  6.5 3.3 copy-start.8
  6.5 3.3 copy-start.6
  6.5 58.9 %all-gather.12.cloned.1.call-start = ((), (), s32[]{:S(2)}) async-start(), calls=%async_computation.5 | async-start | bytes 1179648 | tf_op jit(solution)/shard_map/all_gather | solution.py:13
  9.9 14.1 %copy-start.12 = (u32[32]{0:T(128)S(1)}, u32[32]{0:T(128)}, u32[]{:S(2)}) copy-start(u32[32]{0:T(128)} %constant.125) | copy-start | bytes 388
  21.2 0.7 copy-start
  21.2 1.5 copy-start.3
  21.8 84.4 %all-gather.14.cloned.1.call-start = ((), (), s32[]{:S(2)}) async-start(), calls=%async_computation.6 | async-start | bytes 1179648 | tf_op jit(solution)/shard_map/all_gather | solution.py:169
  22.6 119.7 %reduce-scatter.3.cloned.1.call-start = ((), (), s32[]{:S(2)}) async-start(), calls=%async_computation.3 | async-start | bytes 2621440 | tf_op jit(solution)/shard_map/reduce_scatter | solution.py:174
  22.7 86.0 %copy-start.4 = (f32[2,2,256,128]{3,2,0,1:T(8,128)S(1)}, f32[2,2,256,128]{3,2,0,1:T(8,128)}, u32[]{:S(2)}) copy-start(f32[2,2,256,128]{3,2,0,1:T(8,128)} %copy-done.3) | copy-start | bytes 1572868
  108.9 33.3 %copy-start.1 = (bf16[128,2048]{1,0:T(8,128)(2,1)S(1)}, bf16[128,2048]{1,0:T(8,128)(2,1)}, u32[]{:S(2)}) copy-start(bf16[128,2048]{1,0:T(8,128)(2,1)} %param.24) | copy-start | bytes 1572868
  110.1 33.5 %copy-start.7 = (f32[2048]{0:T(1024)S(1)}, f32[2048]{0:T(1024)}, u32[]{:S(2)}) copy-start(f32[2048]{0:T(1024)} %param.26) | copy-start | bytes 24580
  112.2 110.4 %all-gather.10.cloned.1.call-start = ((), (), s32[]{:S(2)}) async-start(), calls=%async_computation.4 | async-start | bytes 6553600 | tf_op jit(solution)/shard_map/all_gather | solution.py:195
  184.0 168.9 %all-reduce.7.cloned.1.call-start = ((), (), s32[]{:S(2)}) async-start(), calls=%async_computation.7 | async-start | bytes 10485760
  250.1 0.7 copy-start.11
  250.2 111.4 %copy-start.10 = (f32[128,2]{0,1:T(2,128)S(1)}, f32[128,2]{0,1:T(2,128)}, u32[]{:S(2)}) copy-start(f32[128,2]{0,1:T(2,128)} %param.31) | copy-start | bytes 3076
  356.1 36.5 %all-to-all-start.1 = ((bf16[8,1,40,2048]{3,2,1,0:T(8,128)(2,1)}), bf16[8,1,40,2048]{3,2,1,0:T(8,128)(2,1)S(1)}, u32[]{:S(2)}, u32[]{:S(2)}) async-start(bf16[8,1,40,2048]{3,2,1,0:T(8,128)(2,1)} %constant_dynamic-slice_fusion.3), calls=%async_computation.2 | async-start | bytes 2621440 | tf_op jit(solution)/shard_map/all_to_all | solution.py:220
  395.0 5.6 %copy-start.2 = (bf16[128,2048]{1,0:T(8,128)(2,1)S(1)}, bf16[128,2048]{1,0:T(8,128)(2,1)}, u32[]{:S(2)}) copy-start(bf16[128,2048]{1,0:T(8,128)(2,1)} %reduce-scatter.3.cloned.1.call-done) | copy-start | bytes 1572868
Sparse Core Ops, SparseCore 0:
  22.0 43.0 all-gather.11
  67.2 38.9 all-gather.13
  112.3 29.8 reduce-scatter.2
  184.1 38.4 all-gather.9
  250.3 102.5 all-reduce.6
